TPU v7x, 32 devices: a whole 2x2x4 slice. The times are simulated.
32 devices in a mesh: sp: 8 (over z, y), dp: 4 (over x, core).
Axes of the slice: x: 2, y: 2, z: 4, core: 2. Of those that a mesh axis runs over, the one named last changes fastest.
Arguments:
- queries: bfloat16 [4, 1024, 1024], P('dp', 'sp'), may hold values from -6 to 6
- keys: bfloat16 [4, 1024, 256], P('dp', 'sp'), may hold values from -6 to 6
- values: bfloat16 [4, 1024, 256], P('dp', 'sp'), may hold values from -6 to 6
- q_gain: float32 [64], replicated, may hold values from 0.55 to 8
- k_gain: float32 [64], replicated, may hold values from 0.55 to 8
- residual: bfloat16 [4, 1024, 2048], P('dp', 'sp'), may hold values from -6 to 6
- out_weight: bfloat16 [1024, 2048], replicated, may hold values from -0.1875 to 0.1875
- mix_gain: float32 [2048], replicated, may hold values from 0.1 to 1.9
- ffn_gain: float32 [2048], replicated, may hold values from 0.1 to 1.9
- post_gain: float32 [2048], replicated, may hold values from 0.1 to 1.9
- expert_ids: int32 [4, 1024, 2], P('dp', 'sp'), may hold values from 0 to 31, all different within a row; in each aligned block of 128 rows (0 to 127, 128 to 255, ..., all dimensions but the last counted through in order) at most 16 rows name the same one
- expert_gate: float32 [4, 1024, 2], P('dp', 'sp'), may hold values from 0.05 to 1
- w_gate: bfloat16 [32, 2048, 512], P(('sp', 'dp')), may hold values from -0.125 to 0.125
- w_up: bfloat16 [32, 2048, 512], P(('sp', 'dp')), may hold values from -0.125 to 0.125
- w_down: bfloat16 [32, 512, 2048], P(('sp', 'dp')), may hold values from -0.25 to 0.25
Outputs:
- result: bfloat16 [4, 1024, 2048], P('dp', 'sp')
Inputs may be any that keep to these rules, and one draw needn't show every extreme that they name: `expert_ids`: each token names 2 different experts; among the 128 tokens of one device no expert is named more than 16 times, and that bound is reached.
All inputs are finite; a program needn't handle non-finite values.
Results may differ from a plain program's by a relative error of at most 0.0085.
The roundings to bfloat16 on the way count: a program that leaves them out, or rounds other values in their place, can miss the bound.
Values may be sent and summed in bfloat16 or wider, within the bound.
A program may use at most 64 MiB of HBM per device.

v0:
```python
import functools

import jax
import jax.numpy as jnp
import numpy as np
from jax import lax
from jax.experimental import pallas as pl
from jax.experimental.pallas import tpu as pltpu
from jax.sharding import PartitionSpec as P

GRID = 64
LANES = 128
eps_norm = 1e-06
theta_base = 10000.0
MESH = pl.DeviceIdType.MESH
f32 = jnp.float32
bf16 = jnp.bfloat16


def tables(rows, head_size):
    half = head_size // 2
    lane = np.arange(LANES) % head_size
    pair = lane // 2
    quarter = head_size // 4
    by_row = pair < quarter
    frequency = theta_base ** (-(4.0 * (pair % quarter)) / head_size)
    sign = np.where(lane % 2 == 0, -1.0, 1.0)
    a_row = np.arange(rows)[:, None] * frequency
    a_col = np.arange(GRID)[:, None] * frequency
    out = (
        np.where(by_row, np.cos(a_row), 0.0),
        np.where(by_row, np.sin(a_row) * sign, 0.0),
        np.where(by_row, 0.0, np.cos(a_col)),
        np.where(by_row, 0.0, np.sin(a_col) * sign),
    )
    return [jnp.asarray(t, f32) for t in out]


def rms(x):
    return x * lax.rsqrt(jnp.mean(x * x, axis=-1, keepdims=True) + eps_norm)


def dot(a, b):
    return jnp.dot(a, b, preferred_element_type=f32)


def kernel(
    n_sp, n_dp, pitch,
    q_ref, k_ref, v_ref, qg_ref, kg_ref, cr_ref, sr_ref, cc_ref, sc_ref,
    res_ref, mix_ref, ffn_ref, post_ref, ids_ref, gate_ref,
    wo_hbm, wg_hbm, wu_hbm, wd_hbm,
    out_ref,
    kbuf, vbuf, att, first, outbox, arrived, returned, pack, comb_hi, comb_lo,
    ids_far, gate_far, rows_own, rows_far, part_own, part_far, x_send, x_recv,
    wo, wg, wu, wd, w_sem,
    ks_send, ks_recv, vs_send, vs_recv, d_send, d_recv, r_send, r_recv,
):
    sp = lax.axis_index("sp")
    dp = lax.axis_index("dp")
    tok, q_width = q_ref.shape
    kv_width = k_ref.shape[1]
    head = qg_ref.shape[1]
    d_model = res_ref.shape[1]
    heads_q, heads_kv = q_width // head, kv_width // head
    group = heads_q // heads_kv

    weights = [
        pltpu.make_async_copy(src, dst, w_sem.at[n])
        for n, (src, dst) in enumerate(((wo_hbm, wo), (wg_hbm, wg), (wu_hbm, wu), (wd_hbm, wd)))
    ]
    for w in weights:
        w.start()

    span = n_sp // 2
    n_half = span * n_dp
    start = sp // span * span
    place_sp = sp % span
    partner = (lax.rem(sp + span, n_sp), dp)
    base = start * n_dp

    def peer(i):
        return start + lax.rem(place_sp + i // n_dp, span), lax.rem(dp + i % n_dp, n_dp)

    def source(i):
        return (
            start + lax.rem(place_sp + span - i // n_dp, span),
            lax.rem(dp + n_dp - i % n_dp, n_dp),
        )

    barrier = pltpu.get_barrier_semaphore()

    def greet(i, c):
        pl.semaphore_signal(barrier, inc=1, device_id=peer(i), device_id_type=MESH)
        return c

    def greet_far(i, c):
        pl.semaphore_signal(
            barrier, inc=1, device_id=(lax.rem(start + span + i, n_sp), dp), device_id_type=MESH
        )
        return c

    lax.fori_loop(1, n_half, greet, 0)
    lax.fori_loop(0, span, greet_far, 0)

    lane = lax.broadcasted_iota(jnp.int32, (tok, LANES), 1)
    even = lane % 2 == 0
    low = lane % (2 * head) < head
    same = (
        lax.broadcasted_iota(jnp.int32, (LANES, LANES), 0) // head
        == lax.broadcasted_iota(jnp.int32, (LANES, LANES), 1) // head
    ).astype(bf16)
    per_dev = tok // GRID
    cos_t = jnp.concatenate(
        [cc_ref[...] + cr_ref[pl.ds(sp * per_dev + u, 1), :] for u in range(per_dev)], axis=0
    )
    sin_t = jnp.concatenate(
        [sc_ref[...] + sr_ref[pl.ds(sp * per_dev + u, 1), :] for u in range(per_dev)], axis=0
    )

    def turn(x, gain):
        x = x.astype(f32)
        square = x * x
        hi = square.astype(bf16)
        lo = (square - hi.astype(f32)).astype(bf16)
        mean = (dot(hi, same) + dot(lo, same)) * (1.0 / head)
        x = x * lax.rsqrt(mean + eps_norm) * gain
        swapped = jnp.where(even, pltpu.roll(x, LANES - 1, 1), pltpu.roll(x, 1, 1))
        return x * cos_t + swapped * sin_t

    k_gain = jnp.concatenate([kg_ref[...]] * (LANES // head), axis=1)
    q_gain = jnp.concatenate([qg_ref[...]] * (LANES // head), axis=1)
    for c in range(kv_width // LANES):
        cols = slice(c * LANES, (c + 1) * LANES)
        kbuf[0, :, cols] = turn(k_ref[:, cols], k_gain).astype(bf16)
    vbuf[0] = v_ref[...]

    pl.semaphore_wait(barrier, n_half - 1 + span)

    def exchange(n, src, dst):
        return pltpu.make_async_remote_copy(
            src, dst, x_send.at[n], x_recv.at[n], device_id=partner, device_id_type=MESH
        )

    tables_far = [exchange(0, ids_ref, ids_far), exchange(1, gate_ref, gate_far)]
    rows_copy = exchange(2, rows_own, rows_far)
    part_copy = exchange(3, part_own, part_far)
    for copy in tables_far:
        copy.start()

    def kv_copies(i):
        to = (lax.rem(sp + i, n_sp), dp)
        return (
            pltpu.make_async_remote_copy(
                kbuf.at[0], kbuf.at[i], ks_send.at[i], ks_recv.at[i], device_id=to, device_id_type=MESH
            ),
            pltpu.make_async_remote_copy(
                v_ref, vbuf.at[i], vs_send.at[i], vs_recv.at[i], device_id=to, device_id_type=MESH
            ),
        )

    def kv_start(i, c):
        a, b = kv_copies(i)
        a.start()
        b.start()
        return c

    lax.fori_loop(1, n_sp, kv_start, 0)

    q_rows = [[] for _ in range(heads_kv)]
    per_chunk = LANES // head
    for c in range(q_width // LANES):
        x = turn(q_ref[:, c * LANES : (c + 1) * LANES], q_gain) * head ** (-0.5)
        for part in range(per_chunk):
            kv = (c * per_chunk + part) // group
            want = kv % per_chunk
            y = x if part == want else pltpu.roll(x, head, 1)
            keep = low if want == 0 else jnp.logical_not(low)
            q_rows[kv].append(jnp.where(keep, y, 0.0).astype(bf16))

    n_slot = n_half * pitch
    e_iota = lax.broadcasted_iota(jnp.int32, (n_half, tok), 0) + base
    before = (
        lax.broadcasted_iota(jnp.int32, (tok, tok), 0) < lax.broadcasted_iota(jnp.int32, (tok, tok), 1)
    ).astype(bf16)
    spread = (
        lax.broadcasted_iota(jnp.int32, (n_slot, n_half), 0) // pitch
        == lax.broadcasted_iota(jnp.int32, (n_slot, n_half), 1)
    ).astype(bf16)
    place = (lax.broadcasted_iota(jnp.int32, (n_slot, tok), 0) % pitch + 1).astype(f32)

    def route(n, ids, gates):
        hit0 = (e_iota == ids[0:1, :]).astype(f32)
        hit1 = (e_iota == ids[1:2, :]).astype(f32)
        hits = hit0 + hit1
        rank = dot(hits.astype(bf16), before)
        mark = (hits * (rank + 1.0)).astype(bf16)
        chosen = dot(spread, mark) == place
        pack[n] = chosen.astype(f32).astype(bf16)
        g = gates[...]
        g_hi = g.astype(bf16).astype(f32)
        g_lo = g - g_hi
        for dst, part in ((comb_hi, g_hi), (comb_lo, g_lo)):
            both = (hit0 * part[0:1, :] + hit1 * part[1:2, :]).astype(bf16)
            dst[n] = jnp.where(chosen, dot(spread, both), 0.0).astype(bf16)

    route(0, ids_ref, gate_ref)
    for copy in tables_far:
        copy.wait()
    route(1, ids_far, gate_far)

    def kv_wait(i, c):
        a, b = kv_copies(i)
        a.wait()
        b.wait()
        return c

    lax.fori_loop(1, n_sp, kv_wait, 0)

    keys = n_sp * tok
    outs = {}
    for kv in range(heads_kv):
        cols = slice(kv // per_chunk * LANES, (kv // per_chunk + 1) * LANES)
        k_all = kbuf[:, :, cols].reshape(keys, LANES)
        v_all = vbuf[:, :, cols].reshape(keys, LANES)
        for part in range(group):
            s = lax.dot_general(
                q_rows[kv][part], k_all, (((1,), (1,)), ((), ())), preferred_element_type=f32
            )
            p = jnp.exp(s - jnp.max(s, axis=-1, keepdims=True))
            total = jnp.sum(p, axis=-1, keepdims=True)
            outs[kv * group + part] = dot(p.astype(bf16), v_all) / total
    for c in range(q_width // LANES):
        piece = None
        for part in range(per_chunk):
            h = c * per_chunk + part
            have = (h // group) % per_chunk
            y = outs[h] if part == have else pltpu.roll(outs[h], head, 1)
            piece = y if piece is None else jnp.where(low, piece, y)
        att[:, c * LANES : (c + 1) * LANES] = piece.astype(bf16)

    weights[0].wait()
    projected = dot(att[...], wo[...])
    mixed = (res_ref[...].astype(f32) + rms(projected) * mix_ref[...]).astype(bf16)
    first[...] = mixed
    rows_own[...] = (rms(mixed.astype(f32)) * ffn_ref[...]).astype(bf16)
    rows_copy.start()

    me = place_sp * n_dp + dp

    def dispatch(n, i):
        to = peer(i)
        return pltpu.make_async_remote_copy(
            outbox.at[n, (to[0] - start) * n_dp + to[1]], arrived.at[n, i],
            d_send.at[n, i], d_recv.at[n, i], device_id=to, device_id_type=MESH,
        )

    def answer(n, i):
        return pltpu.make_async_remote_copy(
            arrived.at[n, i], returned.at[n, me], r_send.at[n, i], r_recv.at[n, i],
            device_id=source(i), device_id_type=MESH,
        )

    def each(make, act, n, lo_, hi_):
        def step(i, c):
            copy = make(n, i)
            copy.start() if act == "start" else copy.wait()
            return c

        lax.fori_loop(max(lo_, 1), hi_, step, 0)

    def send_rows(n, rows):
        outbox[n] = dot(pack[n], rows).astype(bf16).reshape(n_half, pitch, d_model)
        mid = n_half // 2
        each(dispatch, "start", n, mid, n_half)
        each(dispatch, "start", n, 0, mid)
        arrived[n, 0] = outbox[n, me]

    def experts(n, lo_, hi_):
        x = arrived[n, lo_:hi_].reshape((hi_ - lo_) * pitch, d_model)
        gate_value = dot(x, wg[...])
        up_value = dot(x, wu[...])
        hidden = (gate_value / (1.0 + jnp.exp(-gate_value)) * up_value).astype(bf16)
        y = dot(hidden, wd[...]).astype(bf16)
        arrived[n, lo_:hi_] = y.reshape(hi_ - lo_, pitch, d_model)

    def combine(n):
        back = returned[n].reshape(n_slot, d_model)
        dims = (((0,), (0,)), ((), ()))
        total = lax.dot_general(comb_hi[n], back, dims, preferred_element_type=f32)
        return total + lax.dot_general(comb_lo[n], back, dims, preferred_element_type=f32)

    send_rows(0, rows_own[...])
    for w in weights[1:]:
        w.wait()
    rows_copy.wait()
    send_rows(1, rows_far[...])
    each(dispatch, "wait", 0, 0, n_half)
    experts(0, 0, n_half)
    mid = n_half // 2
    for lo_, hi_ in ((mid, n_half), (0, mid)):
        each(dispatch, "wait", 1, lo_, hi_)
        experts(1, lo_, hi_)
        each(answer, "start", 1, lo_, hi_)
    each(answer, "start", 0, 0, n_half)
    for n in (0, 1):
        returned[n, me] = arrived[n, 0]
    each(answer, "wait", 1, 0, n_half)
    part_own[...] = combine(1).astype(bf16)
    part_copy.start()
    each(answer, "wait", 0, 0, n_half)
    near = combine(0)
    part_copy.wait()
    expert_sum = near + part_far[...].astype(f32)
    out_ref[...] = (first[...].astype(f32) + rms(expert_sum) * post_ref[...]).astype(bf16)


def shards(
    queries, keys, values, q_gain, k_gain, residual, out_weight, mix_gain, ffn_gain, post_gain,
    expert_ids, expert_gate, w_gate, w_up, w_down,
):
    n_sp = lax.axis_size("sp")
    n_dp = lax.axis_size("dp")
    n_dev = n_sp * n_dp
    tok = queries.shape[1]
    d_model = residual.shape[2]
    d_exp = w_gate.shape[2]
    head = q_gain.shape[0]
    kv_width = keys.shape[2]
    q_width = queries.shape[2]
    cap = 2 * tok * expert_ids.shape[2] // n_dev
    pitch = -(-cap // 16) * 16
    n_half = n_dev // 2
    n_slot = n_half * pitch
    top = expert_ids.shape[2]
    vmem = pl.BlockSpec(memory_space=pltpu.VMEM)
    hbm = pl.BlockSpec(memory_space=pl.ANY)
    dma = pltpu.SemaphoreType.DMA
    result = pl.pallas_call(
        functools.partial(kernel, n_sp, n_dp, pitch),
        out_shape=jax.ShapeDtypeStruct((tok, d_model), bf16),
        in_specs=[vmem] * 15 + [hbm] * 4,
        out_specs=vmem,
        scratch_shapes=[
            pltpu.VMEM((n_sp, tok, kv_width), bf16),
            pltpu.VMEM((n_sp, tok, kv_width), bf16),
            pltpu.VMEM((tok, q_width), bf16),
            pltpu.VMEM((tok, d_model), bf16),
            pltpu.VMEM((2, n_half, pitch, d_model), bf16),
            pltpu.VMEM((2, n_half, pitch, d_model), bf16),
            pltpu.VMEM((2, n_half, pitch, d_model), bf16),
            pltpu.VMEM((2, n_slot, tok), bf16),
            pltpu.VMEM((2, n_slot, tok), bf16),
            pltpu.VMEM((2, n_slot, tok), bf16),
            pltpu.VMEM((top, tok), jnp.int32),
            pltpu.VMEM((top, tok), f32),
            pltpu.VMEM((tok, d_model), bf16),
            pltpu.VMEM((tok, d_model), bf16),
            pltpu.VMEM((tok, d_model), bf16),
            pltpu.VMEM((tok, d_model), bf16),
            dma((4,)), dma((4,)),
            pltpu.VMEM((q_width, d_model), bf16),
            pltpu.VMEM((d_model, d_exp), bf16),
            pltpu.VMEM((d_model, d_exp), bf16),
            pltpu.VMEM((d_exp, d_model), bf16),
            dma((4,)),
            dma((n_sp,)), dma((n_sp,)), dma((n_sp,)), dma((n_sp,)),
            dma((2, n_half)), dma((2, n_half)), dma((2, n_half)), dma((2, n_half)),
        ],
        compiler_params=pltpu.CompilerParams(
            collective_id=0, has_side_effects=True, vmem_limit_bytes=63000000
        ),
    )(
        queries[0], keys[0], values[0], q_gain[None], k_gain[None],
        *tables(n_sp * tok // GRID, head),
        residual[0], mix_gain[None], ffn_gain[None], post_gain[None],
        expert_ids[0].T, expert_gate[0].T,
        out_weight, w_gate[0], w_up[0], w_down[0],
    )
    return result[None]


def solution(mesh):
    tokens = P("dp", "sp", None)
    experts = P(("sp", "dp"), None, None)
    return jax.shard_map(
        shards,
        mesh=mesh,
        in_specs=(tokens, tokens, tokens, P(), P(), tokens, P(), P(), P(), P(), tokens, tokens,
                  experts, experts, experts),
        out_specs=tokens,
        check_vma=False,
    )
```

profile of v0, /device:TPU:0, one launch (start us, length us, event | category | flops | bytes accessed | tf_op | source)
XLA Modules:
  0.0 120.8 jit_solution(15679879233315263967)
XLA Ops:
  0.0 118.9 %shard_map.181 = bf16[128,2048]{1,0:T(8,128)(2,1)} custom-call(bf16[128,1024]{1,0:T(8,128)(2,1)} %bitcast.24, bf16[128,256]{1,0:T(8,128)(2,1)} %bitcast.25, bf16[128,256]{1,0:T(8,128)(2,1)} %bitcast.26, f32[1,64]{1,0:T(1,128)} %bitcast.32, f32[1,64]{1,0:T(1,128)} %bitcast.33, f32[16,128]{1,0:T(8,128)} %constant.8.clone.cr_ref, ...), custom_call_target="tpu_custom_call" | custom-call | tf_op jit(solution)/shard_map/pallas_call | solution.py:338
  118.9 1.9 %copy.21 = bf16[1,128,2048]{2,1,0:T(8,128)(2,1)} copy(bf16[1,128,2048]{2,1,0:T(8,128)(2,1)} %bitcast.19) | data formatting | bytes 1048576
where the time goes:
time: 121 us
  Pallas kernels  119 us (98%)
  local copies, waits for them, and re-layouts  1.88 us (2%)
    pallas_call x1, Pallas kernels, shards(): pl.pallas_call(functools.partial(kernel, n_sp, n_dp, pitch), out_shape=ja...  119 us

commit v1 on v0

v1 whole, which is shorter than its diff:
```python
import functools

import jax
import jax.numpy as jnp
import numpy as np
from jax import lax
from jax.experimental import pallas as pl
from jax.experimental.pallas import tpu as pltpu
from jax.sharding import PartitionSpec as P

GRID = 64
LANES = 128
eps_norm = 1e-06
theta_base = 10000.0
MESH = pl.DeviceIdType.MESH
f32 = jnp.float32
bf16 = jnp.bfloat16


def tables(rows, head_size):
    half = head_size // 2
    lane = np.arange(LANES) % head_size
    pair = lane // 2
    quarter = head_size // 4
    by_row = pair < quarter
    frequency = theta_base ** (-(4.0 * (pair % quarter)) / head_size)
    sign = np.where(lane % 2 == 0, -1.0, 1.0)
    a_row = np.arange(rows)[:, None] * frequency
    a_col = np.arange(GRID)[:, None] * frequency
    out = (
        np.where(by_row, np.cos(a_row), 0.0),
        np.where(by_row, np.sin(a_row) * sign, 0.0),
        np.where(by_row, 0.0, np.cos(a_col)),
        np.where(by_row, 0.0, np.sin(a_col) * sign),
    )
    return [jnp.asarray(t, f32) for t in out]


def rms(x):
    return x * lax.rsqrt(jnp.mean(x * x, axis=-1, keepdims=True) + eps_norm)


def dot(a, b):
    return jnp.dot(a, b, preferred_element_type=f32)


def kernel(
    n_sp, n_dp, pitch, n_col,
    q_ref, k_ref, v_ref, qg_ref, kg_ref, cr_ref, sr_ref, cc_ref, sc_ref,
    res_ref, mix_ref, ffn_ref, post_ref, ids_ref, gate_ref,
    wo_hbm, wg_hbm, wu_hbm, wd_hbm,
    out_ref,
    kbuf, vbuf, att, first, rows, outbox, arrived, returned, pack, comb_hi, comb_lo,
    ids_far, gate_far, part, relayed, incoming, total,
    wo, wg, wu, wd, w_sem,
    kz_send, ky_send, k_recv, t_send, t_recv, z_send, z_recv,
    d_send, d_recv, r_send, r_recv, p_send, m_recv, i_recv,
):
    sp = lax.axis_index("sp")
    dp = lax.axis_index("dp")
    tok, q_width = q_ref.shape
    kv_width = k_ref.shape[1]
    head = qg_ref.shape[1]
    d_model = res_ref.shape[1]
    heads_q, heads_kv = q_width // head, kv_width // head
    group = heads_q // heads_kv

    weights = [
        pltpu.make_async_copy(src, dst, w_sem.at[n])
        for n, (src, dst) in enumerate(((wo_hbm, wo), (wg_hbm, wg), (wu_hbm, wu), (wd_hbm, wd)))
    ]
    for w in weights:
        w.start()

    wide = n_dp // 2
    planes = n_sp // wide
    n_pl = wide * n_dp
    n_slot = n_pl * pitch
    cols_c = d_model // n_col
    z = sp // wide
    y = sp % wide
    mid = (z // 2 + z % 2) % 2
    near = z + 1 - 2 * (z % 2)
    across = (z + 2) % planes
    mirror = planes - 1 - z
    is_mid = mid == 1
    is_end = mid == 0

    def at(plane):
        return plane * wide + y, dp

    def peer(i):
        return z * wide + lax.rem(y + i // n_dp, wide), lax.rem(dp + i % n_dp, n_dp)

    def source(i):
        return z * wide + lax.rem(y + wide - i // n_dp, wide), lax.rem(dp + n_dp - i % n_dp, n_dp)

    def remote(src, dst, s_sem, r_sem, to):
        return pltpu.make_async_remote_copy(src, dst, s_sem, r_sem, device_id=to, device_id_type=MESH)

    barrier = pltpu.get_barrier_semaphore()
    up_ok, down_ok = z < planes - 1, z > 0

    @pl.when(up_ok)
    def _():
        pl.semaphore_signal(barrier, inc=1, device_id=at(z + 1), device_id_type=MESH)

    @pl.when(down_ok)
    def _():
        pl.semaphore_signal(barrier, inc=1, device_id=at(z - 1), device_id_type=MESH)

    def greet(i, c):
        pl.semaphore_signal(barrier, inc=1, device_id=peer(i), device_id_type=MESH)
        return c

    lax.fori_loop(1, n_pl, greet, 0)

    lane = lax.broadcasted_iota(jnp.int32, (tok, LANES), 1)
    even = lane % 2 == 0
    low = lane % (2 * head) < head
    same = (
        lax.broadcasted_iota(jnp.int32, (LANES, LANES), 0) // head
        == lax.broadcasted_iota(jnp.int32, (LANES, LANES), 1) // head
    ).astype(bf16)
    per_dev = tok // GRID
    cos_t = jnp.concatenate(
        [cc_ref[...] + cr_ref[pl.ds(sp * per_dev + u, 1), :] for u in range(per_dev)], axis=0
    )
    sin_t = jnp.concatenate(
        [sc_ref[...] + sr_ref[pl.ds(sp * per_dev + u, 1), :] for u in range(per_dev)], axis=0
    )

    def turn(x, gain):
        x = x.astype(f32)
        square = x * x
        hi = square.astype(bf16)
        lo = (square - hi.astype(f32)).astype(bf16)
        mean = (dot(hi, same) + dot(lo, same)) * (1.0 / head)
        x = x * lax.rsqrt(mean + eps_norm) * gain
        swapped = jnp.where(even, pltpu.roll(x, LANES - 1, 1), pltpu.roll(x, 1, 1))
        return x * cos_t + swapped * sin_t

    k_gain = jnp.concatenate([kg_ref[...]] * (LANES // head), axis=1)
    q_gain = jnp.concatenate([qg_ref[...]] * (LANES // head), axis=1)
    for c in range(kv_width // LANES):
        cols = slice(c * LANES, (c + 1) * LANES)
        kbuf[sp, :, cols] = turn(k_ref[:, cols], k_gain).astype(bf16)
    vbuf[sp] = v_ref[...]

    pl.semaphore_wait(barrier, n_pl - 1 + jnp.minimum(z, 1) + jnp.minimum(planes - 1 - z, 1))

    bufs = (kbuf, vbuf)

    def block(kv, plane, own):
        return v_ref if own and kv == 1 else bufs[kv].at[plane * wide + y]

    def along(kv, up, t):
        plane, to = (z - (t - 1), z + 1) if up else (z + (t - 1), z - 1)
        return remote(
            block(kv, plane, t == 1), bufs[kv].at[plane * wide + y],
            kz_send.at[kv, up, t], k_recv.at[kv, plane * wide + y], at(to),
        )

    def aside(kv, plane, j, own=False):
        return remote(
            block(kv, plane, own), bufs[kv].at[plane * wide + y],
            ky_send.at[kv, plane, j], k_recv.at[kv, plane * wide + y],
            (z * wide + lax.rem(y + j, wide), dp),
        )

    def landed(kv, where):
        ref = bufs[kv].at[where]
        remote(ref, ref, kz_send.at[kv, 0, 0], k_recv.at[kv, where], at(z)).wait_recv()

    def along_ok(up, t):
        return (z >= t - 1) & up_ok if up else (z + t - 1 < planes) & down_ok

    def along_start(kv, up, t):
        @pl.when(along_ok(up, t))
        def _():
            along(kv, up, t).start()

    for kv in (1, 0):
        along_start(kv, 1, 1)
        along_start(kv, 0, 1)
        for j in range(1, wide):
            aside(kv, z, j, own=True).start()

    q_rows = [[] for _ in range(heads_kv)]
    per_chunk = LANES // head

    def turn_q(c):
        x = turn(q_ref[:, c * LANES : (c + 1) * LANES], q_gain) * head ** (-0.5)
        for part_ in range(per_chunk):
            kv = (c * per_chunk + part_) // group
            want = kv % per_chunk
            yq = x if part_ == want else pltpu.roll(x, head, 1)
            keep = low if want == 0 else jnp.logical_not(low)
            q_rows[kv].append(jnp.where(keep, yq, 0.0).astype(bf16))

    order = lax.broadcasted_iota(jnp.int32, (n_pl, tok), 0)
    e_iota = z * n_pl + (y + order // n_dp) % wide * n_dp + (dp + order % n_dp) % n_dp
    before = (
        lax.broadcasted_iota(jnp.int32, (tok, tok), 0) < lax.broadcasted_iota(jnp.int32, (tok, tok), 1)
    ).astype(bf16)
    spread = (
        lax.broadcasted_iota(jnp.int32, (n_slot, n_pl), 0) // pitch
        == lax.broadcasted_iota(jnp.int32, (n_slot, n_pl), 1)
    ).astype(bf16)
    place = (lax.broadcasted_iota(jnp.int32, (n_slot, tok), 0) % pitch + 1).astype(f32)

    def route(n, ids, gates):
        hit0 = (e_iota == ids[0:1, :]).astype(f32)
        hit1 = (e_iota == ids[1:2, :]).astype(f32)
        hits = hit0 + hit1
        rank = dot(hits.astype(bf16), before)
        mark = (hits * (rank + 1.0)).astype(bf16)
        chosen = dot(spread, mark) == place
        pack[n] = chosen.astype(f32).astype(bf16)
        g_hi = gates.astype(bf16).astype(f32)
        g_lo = gates - g_hi
        for dst, piece_ in ((comb_hi, g_hi), (comb_lo, g_lo)):
            both = (hit0 * piece_[0:1, :] + hit1 * piece_[1:2, :]).astype(bf16)
            dst[n] = jnp.where(chosen, dot(spread, both), 0.0).astype(bf16)

    n_turn = q_width // LANES
    done = 0
    for t in range(1, planes):
        upto = n_turn * t // (planes - 1)
        for c in range(done, upto):
            turn_q(c)
        done = upto
        if t == planes - 1:
            route(0, ids_ref[...], gate_ref[...])
        for kv in (1, 0):
            for up in (1, 0):
                plane = z - t if up else z + t

                @pl.when((z >= t) if up else (z + t < planes))
                def _():
                    landed(kv, plane * wide + y)
                    if t < planes - 1:
                        along_start(kv, up, t + 1)
                    for j in range(1, wide):
                        aside(kv, plane, j).start()

    def tables_to(n, to):
        return [
            remote(ids_ref, ids_far.at[n], t_send.at[0, n], t_recv.at[0, n], at(to)),
            remote(gate_ref, gate_far.at[n], t_send.at[1, n], t_recv.at[1, n], at(to)),
        ]

    tables_far = [c for n, to in ((1, near), (2, across), (3, mirror)) for c in tables_to(n, to)]
    for copy in tables_far:
        copy.start()

    for kv in (1, 0):
        for plane in range(planes):
            for j in range(1, wide):
                landed(kv, plane * wide + lax.rem(y + wide - j, wide))

    keys = n_sp * tok
    outs = {}
    for kv in range(heads_kv):
        cols = slice(kv // per_chunk * LANES, (kv // per_chunk + 1) * LANES)
        k_all = kbuf[:, :, cols].reshape(keys, LANES)
        v_all = vbuf[:, :, cols].reshape(keys, LANES)
        for part_ in range(group):
            s = lax.dot_general(
                q_rows[kv][part_], k_all, (((1,), (1,)), ((), ())), preferred_element_type=f32
            )
            p = jnp.exp(s - jnp.max(s, axis=-1, keepdims=True))
            denom = jnp.sum(p, axis=-1, keepdims=True)
            outs[kv * group + part_] = dot(p.astype(bf16), v_all) / denom
    for c in range(q_width // LANES):
        piece = None
        for part_ in range(per_chunk):
            h = c * per_chunk + part_
            have = (h // group) % per_chunk
            yo = outs[h] if part_ == have else pltpu.roll(outs[h], head, 1)
            piece = yo if piece is None else jnp.where(low, piece, yo)
        att[:, c * LANES : (c + 1) * LANES] = piece.astype(bf16)

    weights[0].wait()
    projected = dot(att[...], wo[...])
    mixed = (res_ref[...].astype(f32) + rms(projected) * mix_ref[...]).astype(bf16)
    first[...] = mixed
    normed = (rms(mixed.astype(f32)) * ffn_ref[...]).astype(bf16)
    chunks = range(n_col)

    def span(c):
        return slice(c * cols_c, (c + 1) * cols_c)

    for c in chunks:
        rows[0, c] = normed[:, span(c)]

    slots = (0, 1, 2 + mid, 3 - mid)
    beyond = mid * mirror + (1 - mid) * across

    def to_near(c):
        return remote(rows.at[0, c], rows.at[1, c], z_send.at[0, c], z_recv.at[1, c], at(near))

    def to_beyond(c):
        return remote(
            rows.at[0, c], rows.at[slots[2], c], z_send.at[1, c], z_recv.at[slots[2], c], at(beyond)
        )

    def pass_on(s, c):
        return remote(
            rows.at[5 - s, c], rows.at[s, c], z_send.at[s, c], z_recv.at[s, c], at(near)
        )

    def rows_landed(slot, c):
        remote(
            rows.at[slot, c], rows.at[slot, c], z_send.at[0, c], z_recv.at[slot, c], at(near)
        ).wait_recv()

    def relay(s):
        @pl.when(is_mid)
        def _():
            for c in chunks:
                rows_landed(slots[s], c)
                pass_on(s, c).start()

    def dispatch(s, c, i):
        q = slots[s]
        return remote(
            outbox.at[q, c, i], arrived.at[q, c, i], d_send.at[q, c], d_recv.at[q, c], peer(i)
        )

    def answer(s, c, i):
        q = slots[s]
        return remote(
            arrived.at[q, c, i], returned.at[q, c, i], r_send.at[q, c], r_recv.at[q, c], source(i)
        )

    def start_all(make, s, c):
        def step(i, carry):
            make(s, c, i).start()
            return carry

        half = n_pl // 2
        lax.fori_loop(half, n_pl, step, 0)
        lax.fori_loop(1, half, step, 0)

    def others(ref, q, c, s_sem, r_sem):
        ref = ref.at[q, c, 1:n_pl]
        return remote(ref, ref, s_sem.at[q, c], r_sem.at[q, c], at(near))

    def scatter(s):
        q = slots[s]
        for c in chunks:
            if s == 1:
                rows_landed(1, c)
            if s >= 2:
                @pl.when(is_end)
                def _():
                    rows_landed(s, c)

            outbox[q, c] = dot(pack[q], rows[q, c]).astype(bf16).reshape(n_pl, pitch, cols_c)
            start_all(dispatch, s, c)
            arrived[q, c, 0] = outbox[q, c, 0]

    def experts(s):
        q = slots[s]
        gate_value = up_value = None
        for c in chunks:
            others(arrived, q, c, d_send, d_recv).wait_recv()
            x = arrived[q, c].reshape(n_slot, cols_c)
            g, u = dot(x, wg[span(c), :]), dot(x, wu[span(c), :])
            gate_value = g if gate_value is None else gate_value + g
            up_value = u if up_value is None else up_value + u
        hidden = (gate_value / (1.0 + jnp.exp(-gate_value)) * up_value).astype(bf16)
        for c in chunks:
            out = dot(hidden, wd[:, span(c)]).astype(bf16)
            arrived[q, c] = out.reshape(n_pl, pitch, cols_c)
            start_all(answer, s, c)
            returned[q, c, 0] = arrived[q, c, 0]

    def home(s, c):
        return remote(part.at[s, c], incoming.at[min(s, 2) - 1, c], p_send.at[s, c],
                      i_recv.at[min(s, 2) - 1, c], at((None, near, mirror, across)[s]))

    def inward(s, c):
        return remote(part.at[s, c], relayed.at[s - 2, c], p_send.at[s, c],
                      m_recv.at[s - 2, c], at(near))

    dims = (((0,), (0,)), ((), ()))

    def gather(s):
        q = slots[s]
        for c in chunks:
            others(returned, q, c, r_send, r_recv).wait_recv()
            back = returned[q, c].reshape(n_slot, cols_c)
            got = lax.dot_general(comb_hi[q], back, dims, preferred_element_type=f32)
            got = got + lax.dot_general(comb_lo[q], back, dims, preferred_element_type=f32)
            if s == 0:
                total[c] = got
            elif s == 1:
                part[s, c] = got.astype(bf16)
                home(s, c).start()
            else:
                @pl.when(is_end)
                def _():
                    part[s, c] = got.astype(bf16)
                    inward(s, c).start()

                @pl.when(is_mid)
                def _():
                    inward(s, c).wait_recv()
                    part[s, c] = (got + relayed[s - 2, c].astype(f32)).astype(bf16)
                    home(s, c).start()

    for c in chunks:
        to_near(c).start()
    for c in chunks:
        to_beyond(c).start()
    scatter(0)
    for copy in tables_far:
        copy.wait()
    for n in range(1, planes):
        route(n, ids_far[n], gate_far[n])
    for w in weights[1:]:
        w.wait()
    experts(0)
    relay(2)
    scatter(1)
    experts(1)
    gather(0)
    scatter(2)
    relay(3)
    gather(1)
    experts(2)
    scatter(3)
    gather(2)
    experts(3)
    gather(3)

    squares = 0.0
    for c in chunks:
        for n in range(2):
            remote(incoming.at[n, c], incoming.at[n, c], p_send.at[1, c], i_recv.at[n, c], at(near)).wait_recv()
        tot = total[c] + incoming[0, c].astype(f32) + incoming[1, c].astype(f32)
        total[c] = tot
        squares = squares + jnp.sum(tot * tot, axis=-1, keepdims=True)
    scale = lax.rsqrt(squares * (1.0 / d_model) + eps_norm)
    for c in chunks:
        out_ref[:, span(c)] = (
            first[:, span(c)].astype(f32) + total[c] * scale * post_ref[:, span(c)]
        ).astype(bf16)

    for kv in (1, 0):
        for t in range(1, planes):
            for up in (1, 0):
                @pl.when(along_ok(up, t))
                def _():
                    along(kv, up, t).wait_send()

        for plane in range(planes):
            for j in range(1, wide):
                aside(kv, plane, j).wait_send()
    for c in chunks:
        to_near(c).wait_send()
        to_beyond(c).wait_send()

        @pl.when(is_mid)
        def _():
            for s in (2, 3):
                pass_on(s, c).wait_send()

        for s in range(planes):
            others(outbox, s, c, d_send, d_recv).wait_send()
            others(arrived, s, c, r_send, r_recv).wait_send()
            if s:
                home(s, c).wait_send()


def shards(
    queries, keys, values, q_gain, k_gain, residual, out_weight, mix_gain, ffn_gain, post_gain,
    expert_ids, expert_gate, w_gate, w_up, w_down,
):
    n_sp = lax.axis_size("sp")
    n_dp = lax.axis_size("dp")
    n_dev = n_sp * n_dp
    tok = queries.shape[1]
    d_model = residual.shape[2]
    d_exp = w_gate.shape[2]
    head = q_gain.shape[0]
    kv_width = keys.shape[2]
    q_width = queries.shape[2]
    top = expert_ids.shape[2]
    cap = 2 * tok * top // n_dev
    pitch = -(-cap // 16) * 16
    wide = n_dp // 2
    planes = n_sp // wide
    n_pl = wide * n_dp
    n_slot = n_pl * pitch
    n_col = 2
    cols_c = d_model // n_col
    vmem = pl.BlockSpec(memory_space=pltpu.VMEM)
    hbm = pl.BlockSpec(memory_space=pl.ANY)
    dma = pltpu.SemaphoreType.DMA
    result = pl.pallas_call(
        functools.partial(kernel, n_sp, n_dp, pitch, n_col),
        out_shape=jax.ShapeDtypeStruct((tok, d_model), bf16),
        in_specs=[vmem] * 15 + [hbm] * 4,
        out_specs=vmem,
        scratch_shapes=[
            pltpu.VMEM((n_sp, tok, kv_width), bf16),
            pltpu.VMEM((n_sp, tok, kv_width), bf16),
            pltpu.VMEM((tok, q_width), bf16),
            pltpu.VMEM((tok, d_model), bf16),
            pltpu.VMEM((planes, n_col, tok, cols_c), bf16),
            pltpu.VMEM((planes, n_col, n_pl, pitch, cols_c), bf16),
            pltpu.VMEM((planes, n_col, n_pl, pitch, cols_c), bf16),
            pltpu.VMEM((planes, n_col, n_pl, pitch, cols_c), bf16),
            pltpu.VMEM((planes, n_slot, tok), bf16),
            pltpu.VMEM((planes, n_slot, tok), bf16),
            pltpu.VMEM((planes, n_slot, tok), bf16),
            pltpu.VMEM((planes, top, tok), jnp.int32),
            pltpu.VMEM((planes, top, tok), f32),
            pltpu.VMEM((planes, n_col, tok, cols_c), bf16),
            pltpu.VMEM((2, n_col, tok, cols_c), bf16),
            pltpu.VMEM((2, n_col, tok, cols_c), bf16),
            pltpu.VMEM((n_col, tok, cols_c), f32),
            pltpu.VMEM((q_width, d_model), bf16),
            pltpu.VMEM((d_model, d_exp), bf16),
            pltpu.VMEM((d_model, d_exp), bf16),
            pltpu.VMEM((d_exp, d_model), bf16),
            dma((4,)),
            dma((2, 2, planes)), dma((2, planes, wide)), dma((2, n_sp)),
            dma((2, planes)), dma((2, planes)),
            dma((planes, n_col)), dma((planes, n_col)),
            dma((planes, n_col)), dma((planes, n_col)), dma((planes, n_col)), dma((planes, n_col)),
            dma((planes, n_col)), dma((2, n_col)), dma((2, n_col)),
        ],
        compiler_params=pltpu.CompilerParams(
            collective_id=0, has_side_effects=True, vmem_limit_bytes=63000000
        ),
    )(
        queries[0], keys[0], values[0], q_gain[None], k_gain[None],
        *tables(n_sp * tok // GRID, head),
        residual[0], mix_gain[None], ffn_gain[None], post_gain[None],
        expert_ids[0].T, expert_gate[0].T,
        out_weight, w_gate[0], w_up[0], w_down[0],
    )
    return result[None]


def solution(mesh):
    tokens = P("dp", "sp", None)
    experts = P(("sp", "dp"), None, None)
    return jax.shard_map(
        shards,
        mesh=mesh,
        in_specs=(tokens, tokens, tokens, P(), P(), tokens, P(), P(), P(), P(), tokens, tokens,
                  experts, experts, experts),
        out_specs=tokens,
        check_vma=False,
    )
```

time: 121 us -> 108 us (0.89)
  Pallas kernels: 119 us -> 106 us
    pallas_call x1, Pallas kernels: 119 us -> 106 us  [shards(): pl.pallas_call(functools.partial(kernel, n_sp, n_dp, pitch, n_col), out_s...]
where the time goes in v1:
time: 108 us
  Pallas kernels  106 us (98%)
  local copies, waits for them, and re-layouts  1.88 us (2%)
    pallas_call x1, Pallas kernels, shards(): pl.pallas_call(functools.partial(kernel, n_sp, n_dp, pitch, n_col), out_s...  106 us

profile of v1, /device:TPU:0, one launch (start us, length us, event | category | flops | bytes accessed | tf_op | source)
XLA Modules:
  0.0 108.0 jit_solution(8408758376008276169)
XLA Ops:
  0.0 106.1 %shard_map.181 = bf16[128,2048]{1,0:T(8,128)(2,1)} custom-call(bf16[128,1024]{1,0:T(8,128)(2,1)} %bitcast.24, bf16[128,256]{1,0:T(8,128)(2,1)} %bitcast.25, bf16[128,256]{1,0:T(8,128)(2,1)} %bitcast.26, f32[1,64]{1,0:T(1,128)} %bitcast.32, f32[1,64]{1,0:T(1,128)} %bitcast.33, f32[16,128]{1,0:T(8,128)} %constant.8.clone.cr_ref, ...), custom_call_target="tpu_custom_call" | custom-call | tf_op jit(solution)/shard_map/pallas_call | solution.py:503
  106.1 1.9 %copy.21 = bf16[1,128,2048]{2,1,0:T(8,128)(2,1)} copy(bf16[1,128,2048]{2,1,0:T(8,128)(2,1)} %bitcast.19) | data formatting | bytes 1048576

commit v2 on v1

--- a/solution.py
+++ b/solution.py
@@ -46,16 +46,21 @@
 
 def kernel(
     n_sp, n_dp, pitch, n_col,
-    q_ref, k_ref, v_ref, qg_ref, kg_ref, cr_ref, sr_ref, cc_ref, sc_ref,
-    res_ref, mix_ref, ffn_ref, post_ref, ids_ref, gate_ref,
-    wo_hbm, wg_hbm, wu_hbm, wd_hbm,
-    out_ref,
-    kbuf, vbuf, att, first, rows, outbox, arrived, returned, pack, comb_hi, comb_lo,
-    ids_far, gate_far, part, relayed, incoming, total,
-    wo, wg, wu, wd, w_sem,
-    kz_send, ky_send, k_recv, t_send, t_recv, z_send, z_recv,
-    d_send, d_recv, r_send, r_recv, p_send, m_recv, i_recv,
+    *refs,
 ):
+    n_in = 19
+    in_hbm, out_ref, in_vmem, refs = refs[:n_in], refs[n_in], refs[n_in + 1 : 2 * n_in + 1], refs[2 * n_in + 1 :]
+    (
+        k_ref, kg_ref, cr_ref, sr_ref, cc_ref, sc_ref, v_ref, q_ref, qg_ref, ids_ref, gate_ref,
+        res_ref, mix_ref, ffn_ref, post_ref, wo, wg, wu, wd,
+    ) = in_vmem
+    (
+        kbuf, vbuf, att, first, rows, outbox, arrived, returned, pack, comb_hi, comb_lo,
+        ids_far, gate_far, part, relayed, incoming, total, inner, hidden, held,
+        w_sem,
+        kz_send, ky_send, k_recv, t_send, t_recv, z_send, z_recv,
+        d_send, d_recv, r_send, r_recv, p_send, m_recv, i_recv,
+    ) = refs
     sp = lax.axis_index("sp")
     dp = lax.axis_index("dp")
     tok, q_width = q_ref.shape
@@ -64,13 +69,6 @@
     d_model = res_ref.shape[1]
     heads_q, heads_kv = q_width // head, kv_width // head
     group = heads_q // heads_kv
-
-    weights = [
-        pltpu.make_async_copy(src, dst, w_sem.at[n])
-        for n, (src, dst) in enumerate(((wo_hbm, wo), (wg_hbm, wg), (wu_hbm, wu), (wd_hbm, wd)))
-    ]
-    for w in weights:
-        w.start()
 
     wide = n_dp // 2
     planes = n_sp // wide
@@ -115,6 +113,13 @@
 
     lax.fori_loop(1, n_pl, greet, 0)
 
+    loads = [
+        pltpu.make_async_copy(src, dst, w_sem.at[n]) for n, (src, dst) in enumerate(zip(in_hbm, in_vmem))
+    ]
+    for load in loads:
+        load.start()
+    weights = loads[15:]
+
     lane = lax.broadcasted_iota(jnp.int32, (tok, LANES), 1)
     even = lane % 2 == 0
     low = lane % (2 * head) < head
@@ -122,6 +127,8 @@
         lax.broadcasted_iota(jnp.int32, (LANES, LANES), 0) // head
         == lax.broadcasted_iota(jnp.int32, (LANES, LANES), 1) // head
     ).astype(bf16)
+    for load in loads[:7]:
+        load.wait()
     per_dev = tok // GRID
     cos_t = jnp.concatenate(
         [cc_ref[...] + cr_ref[pl.ds(sp * per_dev + u, 1), :] for u in range(per_dev)], axis=0
@@ -141,6 +148,8 @@
         return x * cos_t + swapped * sin_t
 
     k_gain = jnp.concatenate([kg_ref[...]] * (LANES // head), axis=1)
+    for load in loads[7:11]:
+        load.wait()
     q_gain = jnp.concatenate([qg_ref[...]] * (LANES // head), axis=1)
     for c in range(kv_width // LANES):
         cols = slice(c * LANES, (c + 1) * LANES)
@@ -282,6 +291,8 @@
         att[:, c * LANES : (c + 1) * LANES] = piece.astype(bf16)
 
     weights[0].wait()
+    for load in loads[11:15]:
+        load.wait()
     projected = dot(att[...], wo[...])
     mixed = (res_ref[...].astype(f32) + rms(projected) * mix_ref[...]).astype(bf16)
     first[...] = mixed
@@ -295,14 +306,13 @@
         rows[0, c] = normed[:, span(c)]
 
     slots = (0, 1, 2 + mid, 3 - mid)
-    beyond = mid * mirror + (1 - mid) * across
 
     def to_near(c):
         return remote(rows.at[0, c], rows.at[1, c], z_send.at[0, c], z_recv.at[1, c], at(near))
 
-    def to_beyond(c):
+    def to_mirror(n, c):
         return remote(
-            rows.at[0, c], rows.at[slots[2], c], z_send.at[1, c], z_recv.at[slots[2], c], at(beyond)
+            rows.at[n, c], rows.at[3 - n, c], z_send.at[1 + 3 * n, c], z_recv.at[3 - n, c], at(mirror)
         )
 
     def pass_on(s, c):
@@ -315,12 +325,11 @@
             rows.at[slot, c], rows.at[slot, c], z_send.at[0, c], z_recv.at[slot, c], at(near)
         ).wait_recv()
 
-    def relay(s):
+    def relay(s, c):
         @pl.when(is_mid)
         def _():
-            for c in chunks:
-                rows_landed(slots[s], c)
-                pass_on(s, c).start()
+            rows_landed(slots[s], c)
+            pass_on(s, c).start()
 
     def dispatch(s, c, i):
         q = slots[s]
@@ -347,35 +356,42 @@
         ref = ref.at[q, c, 1:n_pl]
         return remote(ref, ref, s_sem.at[q, c], r_sem.at[q, c], at(near))
 
-    def scatter(s):
+    def scatter(s, c):
         q = slots[s]
-        for c in chunks:
-            if s == 1:
-                rows_landed(1, c)
-            if s >= 2:
-                @pl.when(is_end)
-                def _():
-                    rows_landed(s, c)
-
-            outbox[q, c] = dot(pack[q], rows[q, c]).astype(bf16).reshape(n_pl, pitch, cols_c)
-            start_all(dispatch, s, c)
-            arrived[q, c, 0] = outbox[q, c, 0]
-
-    def experts(s):
+        if s == 1:
+            rows_landed(1, c)
+
+            @pl.when(is_mid)
+            def _():
+                to_mirror(1, c).start()
+
+        if s >= 2:
+            @pl.when(is_end)
+            def _():
+                rows_landed(s, c)
+
+        outbox[q, c] = dot(pack[q], rows[q, c]).astype(bf16).reshape(n_pl, pitch, cols_c)
+        start_all(dispatch, s, c)
+        arrived[q, c, 0] = outbox[q, c, 0]
+
+    def widen(s, c):
         q = slots[s]
-        gate_value = up_value = None
-        for c in chunks:
-            others(arrived, q, c, d_send, d_recv).wait_recv()
-            x = arrived[q, c].reshape(n_slot, cols_c)
-            g, u = dot(x, wg[span(c), :]), dot(x, wu[span(c), :])
-            gate_value = g if gate_value is None else gate_value + g
-            up_value = u if up_value is None else up_value + u
-        hidden = (gate_value / (1.0 + jnp.exp(-gate_value)) * up_value).astype(bf16)
-        for c in chunks:
-            out = dot(hidden, wd[:, span(c)]).astype(bf16)
-            arrived[q, c] = out.reshape(n_pl, pitch, cols_c)
-            start_all(answer, s, c)
-            returned[q, c, 0] = arrived[q, c, 0]
+        others(arrived, q, c, d_send, d_recv).wait_recv()
+        x = arrived[q, c].reshape(n_slot, cols_c)
+        for n, w in enumerate((wg, wu)):
+            got = dot(x, w[span(c), :])
+            inner[s % 2, n] = got if c == 0 else inner[s % 2, n] + got
+
+    def hide(s):
+        gate_value, up_value = inner[s % 2, 0], inner[s % 2, 1]
+        hidden[s % 2] = (gate_value / (1.0 + jnp.exp(-gate_value)) * up_value).astype(bf16)
+
+    def narrow(s, c):
+        q = slots[s]
+        out = dot(hidden[s % 2], wd[:, span(c)]).astype(bf16)
+        arrived[q, c] = out.reshape(n_pl, pitch, cols_c)
+        start_all(answer, s, c)
+        returned[q, c, 0] = arrived[q, c, 0]
 
     def home(s, c):
         return remote(part.at[s, c], incoming.at[min(s, 2) - 1, c], p_send.at[s, c],
@@ -387,54 +403,130 @@
 
     dims = (((0,), (0,)), ((), ()))
 
-    def gather(s):
+    def gather(s, c):
         q = slots[s]
-        for c in chunks:
-            others(returned, q, c, r_send, r_recv).wait_recv()
-            back = returned[q, c].reshape(n_slot, cols_c)
-            got = lax.dot_general(comb_hi[q], back, dims, preferred_element_type=f32)
-            got = got + lax.dot_general(comb_lo[q], back, dims, preferred_element_type=f32)
-            if s == 0:
-                total[c] = got
-            elif s == 1:
+        others(returned, q, c, r_send, r_recv).wait_recv()
+        back = returned[q, c].reshape(n_slot, cols_c)
+        got = lax.dot_general(comb_hi[q], back, dims, preferred_element_type=f32)
+        got = got + lax.dot_general(comb_lo[q], back, dims, preferred_element_type=f32)
+        if s == 0:
+            total[c] = got
+        elif s == 1:
+            part[s, c] = got.astype(bf16)
+            home(s, c).start()
+        else:
+            @pl.when(is_end)
+            def _():
                 part[s, c] = got.astype(bf16)
-                home(s, c).start()
-            else:
-                @pl.when(is_end)
-                def _():
-                    part[s, c] = got.astype(bf16)
-                    inward(s, c).start()
-
-                @pl.when(is_mid)
-                def _():
-                    inward(s, c).wait_recv()
-                    part[s, c] = (got + relayed[s - 2, c].astype(f32)).astype(bf16)
-                    home(s, c).start()
+                inward(s, c).start()
+
+            @pl.when(is_mid)
+            def _():
+                held[s - 2, c] = got
+
+    def merge(s, c):
+        @pl.when(is_mid)
+        def _():
+            inward(s, c).wait_recv()
+            part[s, c] = (held[s - 2, c] + relayed[s - 2, c].astype(f32)).astype(bf16)
+            home(s, c).start()
 
     for c in chunks:
         to_near(c).start()
+
+    @pl.when(is_mid)
+    def _():
+        for c in chunks:
+            to_mirror(0, c).start()
+
     for c in chunks:
-        to_beyond(c).start()
-    scatter(0)
+        scatter(0, c)
     for copy in tables_far:
         copy.wait()
     for n in range(1, planes):
         route(n, ids_far[n], gate_far[n])
     for w in weights[1:]:
         w.wait()
-    experts(0)
-    relay(2)
-    scatter(1)
-    experts(1)
-    gather(0)
-    scatter(2)
-    relay(3)
-    gather(1)
-    experts(2)
-    scatter(3)
-    gather(2)
-    experts(3)
-    gather(3)
+    relay(2, 1)
+    widen(0, 0)
+    scatter(1, 0)
+    scatter(1, 1)
+    widen(0, 1)
+    widen(0, 2)
+    widen(0, 3)
+    hide(0)
+    narrow(0, 2)
+    relay(2, 0)
+    widen(1, 0)
+    scatter(1, 2)
+    narrow(0, 3)
+    widen(1, 1)
+    relay(2, 2)
+    scatter(1, 3)
+    relay(2, 3)
+    narrow(0, 0)
+    widen(1, 2)
+    relay(3, 0)
+    scatter(2, 1)
+    relay(3, 1)
+    widen(1, 3)
+    narrow(0, 1)
+    hide(1)
+    narrow(1, 3)
+    scatter(2, 0)
+    gather(0, 3)
+    narrow(1, 2)
+    scatter(2, 2)
+    relay(3, 2)
+    relay(3, 3)
+    narrow(1, 0)
+    gather(1, 3)
+    scatter(2, 3)
+    gather(1, 2)
+    widen(2, 0)
+    narrow(1, 1)
+    gather(1, 0)
+    scatter(3, 0)
+    gather(0, 2)
+    widen(2, 1)
+    widen(2, 2)
+    widen(2, 3)
+    hide(2)
+    narrow(2, 2)
+    gather(1, 1)
+    scatter(3, 1)
+    widen(3, 0)
+    narrow(2, 3)
+    scatter(3, 2)
+    narrow(2, 0)
+    gather(2, 2)
+    widen(3, 1)
+    scatter(3, 3)
+    gather(2, 3)
+    merge(2, 2)
+    narrow(2, 1)
+    merge(2, 3)
+    gather(0, 0)
+    gather(2, 0)
+    gather(0, 1)
+    merge(2, 0)
+    widen(3, 2)
+    widen(3, 3)
+    hide(3)
+    narrow(3, 0)
+    gather(2, 1)
+    narrow(3, 1)
+    merge(2, 1)
+    narrow(3, 2)
+    gather(3, 0)
+    merge(3, 0)
+    gather(3, 1)
+    narrow(3, 3)
+    merge(3, 1)
+    gather(3, 2)
+    gather(3, 3)
+    merge(3, 2)
+    merge(3, 3)
 
     squares = 0.0
     for c in chunks:
@@ -461,10 +553,11 @@
                 aside(kv, plane, j).wait_send()
     for c in chunks:
         to_near(c).wait_send()
-        to_beyond(c).wait_send()
 
         @pl.when(is_mid)
         def _():
+            for n in (0, 1):
+                to_mirror(n, c).wait_send()
             for s in (2, 3):
                 pass_on(s, c).wait_send()
 
@@ -495,17 +588,23 @@
     planes = n_sp // wide
     n_pl = wide * n_dp
     n_slot = n_pl * pitch
-    n_col = 2
+    n_col = 4
     cols_c = d_model // n_col
     vmem = pl.BlockSpec(memory_space=pltpu.VMEM)
     hbm = pl.BlockSpec(memory_space=pl.ANY)
     dma = pltpu.SemaphoreType.DMA
+    rows_t, rows_s, cols_t, cols_s = tables(n_sp * tok // GRID, head)
+    operands = (
+        keys[0], k_gain[None], rows_t, rows_s, cols_t, cols_s, values[0], queries[0], q_gain[None],
+        expert_ids[0].T, expert_gate[0].T, residual[0], mix_gain[None], ffn_gain[None], post_gain[None],
+        out_weight, w_gate[0], w_up[0], w_down[0],
+    )
     result = pl.pallas_call(
         functools.partial(kernel, n_sp, n_dp, pitch, n_col),
         out_shape=jax.ShapeDtypeStruct((tok, d_model), bf16),
-        in_specs=[vmem] * 15 + [hbm] * 4,
+        in_specs=[hbm] * len(operands),
         out_specs=vmem,
-        scratch_shapes=[
+        scratch_shapes=[pltpu.VMEM(x.shape, x.dtype) for x in operands] + [
             pltpu.VMEM((n_sp, tok, kv_width), bf16),
             pltpu.VMEM((n_sp, tok, kv_width), bf16),
             pltpu.VMEM((tok, q_width), bf16),
@@ -523,27 +622,20 @@
             pltpu.VMEM((2, n_col, tok, cols_c), bf16),
             pltpu.VMEM((2, n_col, tok, cols_c), bf16),
             pltpu.VMEM((n_col, tok, cols_c), f32),
-            pltpu.VMEM((q_width, d_model), bf16),
-            pltpu.VMEM((d_model, d_exp), bf16),
-            pltpu.VMEM((d_model, d_exp), bf16),
-            pltpu.VMEM((d_exp, d_model), bf16),
-            dma((4,)),
+            pltpu.VMEM((2, 2, n_slot, d_exp), f32),
+            pltpu.VMEM((2, n_slot, d_exp), bf16),
+            pltpu.VMEM((2, n_col, tok, cols_c), f32),
+            dma((len(operands),)),
             dma((2, 2, planes)), dma((2, planes, wide)), dma((2, n_sp)),
             dma((2, planes)), dma((2, planes)),
-            dma((planes, n_col)), dma((planes, n_col)),
+            dma((planes + 1, n_col)), dma((planes, n_col)),
             dma((planes, n_col)), dma((planes, n_col)), dma((planes, n_col)), dma((planes, n_col)),
             dma((planes, n_col)), dma((2, n_col)), dma((2, n_col)),
         ],
         compiler_params=pltpu.CompilerParams(
             collective_id=0, has_side_effects=True, vmem_limit_bytes=63000000
         ),
-    )(
-        queries[0], keys[0], values[0], q_gain[None], k_gain[None],
-        *tables(n_sp * tok // GRID, head),
-        residual[0], mix_gain[None], ffn_gain[None], post_gain[None],
-        expert_ids[0].T, expert_gate[0].T,
-        out_weight, w_gate[0], w_up[0], w_down[0],
-    )
+    )(*operands)
     return result[None]
 
 

time: 108 us -> 94.4 us (0.87)
  Pallas kernels: 106 us -> 92.4 us
    pallas_call x1, Pallas kernels: 106 us -> 92.4 us  [shards(): pl.pallas_call(functools.partial(kernel, n_sp, n_dp, pitch, n_col), out_s...]
where the time goes in v2:
time: 94.4 us; the launch traced here: 94.3 us
  Pallas kernels  92.4 us (98%)
  local copies, waits for them, and re-layouts  1.88 us (2%)
    pallas_call x1, Pallas kernels, shards(): pl.pallas_call(functools.partial(kernel, n_sp, n_dp, pitch, n_col), out_s...  92.4 us

profile of v2, /device:TPU:0, one launch (start us, length us, event | category | flops | bytes accessed | tf_op | source)
XLA Modules:
  0.0 94.3 jit_solution(11689375618591466951)
XLA Ops:
  0.0 92.4 %shard_map.181 = bf16[128,2048]{1,0:T(8,128)(2,1)} custom-call(bf16[128,256]{1,0:T(8,128)(2,1)} %bitcast.25, f32[1,64]{1,0:T(1,128)} %bitcast.32, f32[16,128]{1,0:T(8,128)} %constant.8.clone.refs_2_, f32[16,128]{1,0:T(8,128)} %constant.9.clone.refs_3_, f32[64,128]{1,0:T(8,128)} %constant.10.clone.refs_4_, f32[64,128]{1,0:T(8,128)} %constant.11.clone.refs_5_, ...), custom_call_target="tpu_custom_call" | custom-call | tf_op jit(solution)/shard_map/pallas_call | solution.py:602
  92.4 1.9 %copy.21 = bf16[1,128,2048]{2,1,0:T(8,128)(2,1)} copy(bf16[1,128,2048]{2,1,0:T(8,128)(2,1)} %bitcast.19) | data formatting | bytes 1048576

commit v3 on v2

--- a/solution.py
+++ b/solution.py
@@ -269,18 +269,21 @@
                 landed(kv, plane * wide + lax.rem(y + wide - j, wide))
 
     keys = n_sp * tok
+    many = group if group * tok * keys <= 1 << 19 else 1
     outs = {}
     for kv in range(heads_kv):
         cols = slice(kv // per_chunk * LANES, (kv // per_chunk + 1) * LANES)
         k_all = kbuf[:, :, cols].reshape(keys, LANES)
         v_all = vbuf[:, :, cols].reshape(keys, LANES)
-        for part_ in range(group):
+        for first_ in range(0, group, many):
+            q_all = jnp.concatenate(q_rows[kv][first_ : first_ + many], axis=0)
             s = lax.dot_general(
-                q_rows[kv][part_], k_all, (((1,), (1,)), ((), ())), preferred_element_type=f32
+                q_all, k_all, (((1,), (1,)), ((), ())), preferred_element_type=f32
             )
             p = jnp.exp(s - jnp.max(s, axis=-1, keepdims=True))
-            denom = jnp.sum(p, axis=-1, keepdims=True)
-            outs[kv * group + part_] = dot(p.astype(bf16), v_all) / denom
+            out = dot(p.astype(bf16), v_all) / jnp.sum(p, axis=-1, keepdims=True)
+            for n in range(many):
+                outs[kv * group + first_ + n] = out[n * tok : (n + 1) * tok]
     for c in range(q_width // LANES):
         piece = None
         for part_ in range(per_chunk):

time: 94.4 us -> 91.9 us (0.974)
  Pallas kernels: 92.4 us -> 89.9 us
    pallas_call x1, Pallas kernels: 92.4 us -> 89.9 us  [shards(): pl.pallas_call(functools.partial(kernel, n_sp, n_dp, pitch, n_col), out_s...]
where the time goes in v3:
time: 91.9 us; the launch traced here: 91.8 us
  Pallas kernels  89.9 us (98%)
  local copies, waits for them, and re-layouts  1.88 us (2%)
    pallas_call x1, Pallas kernels, shards(): pl.pallas_call(functools.partial(kernel, n_sp, n_dp, pitch, n_col), out_s...  89.9 us
    unnamed x1, local copies, waits for them, and re-layouts  1.88 us

profile of v3, /device:TPU:0, one launch (start us, length us, event | category | flops | bytes accessed | tf_op | source)
XLA Modules:
  0.0 91.8 jit_solution(10754041082791645188)
XLA Ops:
  0.0 89.9 %shard_map.181 = bf16[128,2048]{1,0:T(8,128)(2,1)} custom-call(bf16[128,256]{1,0:T(8,128)(2,1)} %bitcast.25, f32[1,64]{1,0:T(1,128)} %bitcast.32, f32[16,128]{1,0:T(8,128)} %constant.8.clone.refs_2_, f32[16,128]{1,0:T(8,128)} %constant.9.clone.refs_3_, f32[64,128]{1,0:T(8,128)} %constant.10.clone.refs_4_, f32[64,128]{1,0:T(8,128)} %constant.11.clone.refs_5_, ...), custom_call_target="tpu_custom_call" | custom-call | tf_op jit(solution)/shard_map/pallas_call | solution.py:605
  89.9 1.9 %copy.21 = bf16[1,128,2048]{2,1,0:T(8,128)(2,1)} copy(bf16[1,128,2048]{2,1,0:T(8,128)(2,1)} %bitcast.19) | data formatting | bytes 1048576
